TPU v7x, 32 devices: a whole 2x2x4 slice. The times are simulated.
32 devices in a mesh: sp: 8 (over z, y), dp: 4 (over x, core).
Axes of the slice: x: 2, y: 2, z: 4, core: 2. Of those that a mesh axis runs over, the one named last changes fastest.
Arguments:
- tokens: bfloat16 [4, 2048, 2048], P('dp', 'sp'), may hold values from -6 to 6
- w_query: bfloat16 [2048, 2048], P('dp', 'sp'), may hold values from -0.125 to 0.125
- w_key: bfloat16 [2048, 1024], P('dp', 'sp'), may hold values from -0.125 to 0.125
- w_value: bfloat16 [2048, 1024], P('dp', 'sp'), may hold values from -0.125 to 0.125
- w_out: bfloat16 [2048, 2048], P('dp', 'sp'), may hold values from -0.25 to 0.25
- qk_gain: float32 [2, 128], replicated, may hold values from 0.9 to 24
Outputs:
- mixed_out: bfloat16 [4, 2048, 2048], P('dp', 'sp')
All inputs are finite; a program needn't handle non-finite values.
Results may differ from a plain program's by a relative error of at most 0.006.
The roundings to bfloat16 on the way count: a program that leaves them out, or rounds other values in their place, can miss the bound.
Values may be sent and summed in bfloat16 or wider, within the bound.
A program may use at most 64 MiB of HBM per device.

v0:
```python
import math
import jax
import jax.numpy as jnp
import numpy as np
from jax import lax
from jax.sharding import PartitionSpec as P

HQ = 16
KV = 8
HD = 128
GRID_W = 64
ROPE_BASE = 10000.0
EPS = 1e-06


def angles(positions):
    quarter = jnp.arange(0, HD // 2, 2, dtype=jnp.float32)
    inv_freq = ROPE_BASE ** (-quarter / (HD // 2))
    row_pos = (positions // GRID_W).astype(jnp.float32)
    col_pos = (positions % GRID_W).astype(jnp.float32)
    angle_table = jnp.concatenate(
        [row_pos[:, None] * inv_freq, col_pos[:, None] * inv_freq], axis=1
    )
    return (jnp.cos(angle_table), jnp.sin(angle_table))


def prepare(raw_proj, gain_row, cosine, sine_table):
    normed = (
        raw_proj * lax.rsqrt(jnp.mean(raw_proj * raw_proj, axis=-1, keepdims=True) + EPS) * gain_row
    )
    pair_view = normed.reshape(raw_proj.shape[:-1] + (HD // 2, 2))
    first_half = pair_view[..., 0]
    second = pair_view[..., 1]
    cos_b = cosine[:, None, :]
    sin_b = sine_table[:, None, :]
    turned = jnp.stack(
        [first_half * cos_b - second * sin_b, first_half * sin_b + second * cos_b], axis=-1
    )
    return turned.reshape(raw_proj.shape).astype(jnp.bfloat16)


def attend_head(query_rows, key_rows, value_rows):
    seq_len = query_rows.shape[0]
    block_len = math.gcd(seq_len, 512)
    blocks = query_rows.reshape(seq_len // block_len, block_len, HD)

    def one_block(row_block):
        scores = jnp.dot(row_block, key_rows.T, preferred_element_type=jnp.float32) * HD ** (-0.5)
        top_score = jnp.max(scores, axis=1, keepdims=True)
        weights = jnp.exp(scores - top_score)
        row_total = jnp.sum(weights, axis=1, keepdims=True)
        probs_bf = (weights / row_total).astype(jnp.bfloat16)
        return jnp.dot(probs_bf, value_rows, preferred_element_type=jnp.float32).astype(
            jnp.bfloat16
        )

    return lax.map(one_block, blocks).reshape(seq_len, HD)


def project(own_rows, weight):
    col_full = lax.all_gather(weight, "sp", axis=1, tiled=True)
    return jnp.dot(
        own_rows,
        lax.all_gather(col_full, "dp", axis=0, tiled=True),
        preferred_element_type=jnp.float32,
    )


def on_device(tokens, w_query, w_key, w_value, w_out, qk_gain):
    own_rows = tokens[0]
    n_seqdev = lax.axis_size("sp")
    tok_local = own_rows.shape[0]
    positions = lax.axis_index("sp") * tok_local + jnp.arange(tok_local, dtype=jnp.int32)
    cosine, sine_table = angles(positions)
    heads_dev = HQ // n_seqdev
    group_size = HQ // KV
    kv_dev = max(1, heads_dev // group_size)
    chosen = (np.arange(n_seqdev) * heads_dev // group_size)[:, None] + np.arange(kv_dev)[None, :]
    chosen = chosen.reshape(-1)
    key_all = prepare(
        project(own_rows, w_key).reshape(tok_local, KV, HD), qk_gain[1], cosine, sine_table
    )
    values = project(own_rows, w_value).astype(jnp.bfloat16).reshape(tok_local, KV, HD)
    key_send = key_all[:, chosen, :].reshape(tok_local, -1)
    value_send = values[:, chosen, :].reshape(tok_local, -1)
    raw_proj = project(own_rows, w_query).reshape(tok_local, HQ, HD)
    query_heads = lax.all_to_all(
        prepare(raw_proj, qk_gain[0], cosine, sine_table).reshape(tok_local, HQ * HD),
        "sp",
        split_axis=1,
        concat_axis=0,
        tiled=True,
    )
    key_heads = lax.all_to_all(key_send, "sp", split_axis=1, concat_axis=0, tiled=True)
    value_heads = lax.all_to_all(value_send, "sp", split_axis=1, concat_axis=0, tiled=True)
    outputs = []
    for head_index in range(heads_dev):
        kv_slot = head_index // group_size if heads_dev >= group_size else 0
        outputs.append(
            attend_head(
                query_heads[:, head_index * HD : (head_index + 1) * HD],
                key_heads[:, kv_slot * HD : (kv_slot + 1) * HD],
                value_heads[:, kv_slot * HD : (kv_slot + 1) * HD],
            )
        )
    mixed_heads = jnp.concatenate(outputs, axis=1)
    token_rows = lax.all_to_all(mixed_heads, "sp", split_axis=0, concat_axis=1, tiled=True)
    return project(token_rows, w_out).astype(jnp.bfloat16)[None]


def solution(mesh):
    in_specs = (
        P("dp", "sp", None),
        P("dp", "sp"),
        P("dp", "sp"),
        P("dp", "sp"),
        P("dp", "sp"),
        P(),
    )
    out_specs = P("dp", "sp", None)
    return jax.shard_map(
        on_device, mesh=mesh, in_specs=in_specs, out_specs=out_specs, check_vma=False
    )
```

profile of v0, /device:TPU:0, one launch (start us, length us, event | category | flops | bytes accessed | tf_op | source)
XLA Modules:
  0.0 416.6 jit_solution(12027826076929534750)
XLA Ops:
  8.8 42.7 %all-gather.17.cloned.1.call-done = bf16[512,1024]{1,0:T(8,128)(2,1)} async-done(((bf16[512,128]{1,0:T(8,128)(2,1)}), bf16[512,1024]{1,0:T(8,128)(2,1)}) %all-gather.17.cloned.1.call-update) | async-done | bytes 1048592 | tf_op jit(solution)/shard_map/all_gather | solution.py:61
  51.6 51.4 %all-gather.9.cloned.1.call-done = bf16[512,2048]{1,0:T(8,128)(2,1)} async-done(((bf16[512,256]{1,0:T(8,128)(2,1)}), bf16[512,2048]{1,0:T(8,128)(2,1)}) %all-gather.9.cloned.1.call-update) | async-done | bytes 2097168 | tf_op jit(solution)/shard_map/all_gather | solution.py:61
  103.0 39.6 %all-gather.13.cloned.1.call-done = bf16[512,1024]{1,0:T(8,128)(2,1)} async-done(((bf16[512,128]{1,0:T(8,128)(2,1)}), bf16[512,1024]{1,0:T(8,128)(2,1)}) %all-gather.13.cloned.1.call-update) | async-done | bytes 1048592 | tf_op jit(solution)/shard_map/all_gather | solution.py:61
  143.8 33.7 %all-gather.19.cloned.1.call-done = bf16[2048,1024]{1,0:T(8,128)(2,1)} async-done(((bf16[512,1024]{1,0:T(8,128)(2,1)}), bf16[2048,1024]{1,0:T(8,128)(2,1)}) %all-gather.19.cloned.1.call-update) | async-done | bytes 4194320 | tf_op jit(solution)/shard_map/all_gather | solution.py:64
  177.6 3.4 fusion.21
  182.6 5.5 %all-to-all-start.2 = ((bf16[256,8,128]{2,0,1:T(8,128)(2,1)}), bf16[256,8,128]{2,0,1:T(8,128)(2,1)}, u32[]{:S(2)}, u32[]{:S(2)}) async-start(bf16[256,8,128]{2,0,1:T(8,128)(2,1)} %bitcast.19), calls=%async_computation.2 | async-start | bytes 1048576 | tf_op jit(solution)/shard_map/all_to_all | solution.py:95
  188.1 49.2 %all-gather.11.cloned.1.call-done = bf16[2048,2048]{1,0:T(8,128)(2,1)} async-done(((bf16[512,2048]{1,0:T(8,128)(2,1)}), bf16[2048,2048]{1,0:T(8,128)(2,1)}) %all-gather.11.cloned.1.call-update) | async-done | bytes 8388624 | tf_op jit(solution)/shard_map/all_gather | solution.py:64
  237.3 12.2 %copy.19 = bf16[2048,2048]{1,0:T(8,128)(2,1)} copy(bf16[2048,2048]{0,1:T(8,128)(2,1)} %bitcast.93) | data formatting | bytes 16777216 | tf_op jit(solution)/shard_map/dot_general | solution.py:62
  249.5 5.8 %multiply_reduce_fusion.2 = (f32[256,16]{0,1:T(8,128)S(1)}, f32[256,16,128]{0,2,1:T(8,128)S(1)}) fusion(bf16[16,128,2048]{2,1,0:T(8,128)(2,1)} %bitcast.94, bf16[1,256,2048]{2,1,0:T(8,128)(2,1)S(1)} %copy-done), kind=kOutput, calls=%fused_computation.31 | convolution fusion | flops 2148528128 | bytes 11550720 | tf_op jit(solution)/shard_map/dot_general | solution.py:62
  257.0 2.5 reshape.165
  259.5 2.9 subtract_convert_fusion
  262.4 2.4 pad_maximum_fusion
  266.1 5.5 %all-to-all-start = ((bf16[256,8,256]{0,2,1:T(8,128)(2,1)}), bf16[256,8,256]{0,2,1:T(8,128)(2,1)S(1)}, u32[]{:S(2)}, u32[]{:S(2)}) async-start(bf16[256,8,256]{0,2,1:T(8,128)(2,1)} %convert_element_type.44), calls=%async_computation | async-start | bytes 2097152 | tf_op jit(solution)/shard_map/all_to_all | solution.py:87
  273.2 6.5 %copy.21 = bf16[1024,2048]{1,0:T(8,128)(2,1)} copy(bf16[1024,2048]{0,1:T(8,128)(2,1)} %bitcast.96) | data formatting | bytes 8388608 | tf_op jit(solution)/shard_map/dot_general | solution.py:62
  279.7 3.5 multiply_reduce_fusion.3
  286.1 20.1 %all-to-all-done = bf16[256,8,256]{0,2,1:T(8,128)(2,1)S(1)} async-done(((bf16[256,8,256]{0,2,1:T(8,128)(2,1)}), bf16[256,8,256]{0,2,1:T(8,128)(2,1)S(1)}, u32[]{:S(2)}, u32[]{:S(2)}) %all-to-all-start) | async-done | bytes 1048608 | tf_op jit(solution)/shard_map/all_to_all | solution.py:87
  306.2 3.5 all-to-all-start.1
  309.8 31.3 %all-gather.21.cloned.1.call-done = bf16[512,2048]{1,0:T(8,128)(2,1)} async-done(((bf16[512,256]{1,0:T(8,128)(2,1)}), bf16[512,2048]{1,0:T(8,128)(2,1)}) %all-gather.21.cloned.1.call-update) | async-done | bytes 2097168 | tf_op jit(solution)/shard_map/all_gather | solution.py:61
  341.8 15.1 %while.21 = (s32[]{:T(128)}, bf16[4,512,128]{2,1,0:T(8,128)(2,1)S(1)}, bf16[4,512,128]{2,1,0:T(8,128)(2,1)S(1)}, bf16[2048,128]{1,0:T(8,128)(2,1)S(1)}, bf16[2048,128]{1,0:T(8,128)(2,1)}, /*index=5*/s32[]{:T(128)}) while((s32[]{:T(128)}, bf16[4,512,128]{2,1,0:T(8,128)(2,1)S(1)}, bf16[4,512,128]{2,1,0:T(8,128)(2,1)S(1)}, ...), condition=%wide.region_9.10_spmd, body=%wide.region_6.9_spmd.sunk | while | flops 546372608 | bytes 13903957 | solution.py:57
  347.2 2.2 fusion.57
  350.9 2.2 fusion.57
  357.0 14.9 %while.20 = (s32[]{:T(128)}, bf16[4,512,128]{2,1,0:T(8,128)(2,1)S(1)}, bf16[4,512,128]{2,1,0:T(8,128)(2,1)S(1)}, bf16[2048,128]{1,0:T(8,128)(2,1)S(1)}, bf16[2048,128]{1,0:T(8,128)(2,1)}, /*index=5*/s32[]{:T(128)}) while((s32[]{:T(128)}, bf16[4,512,128]{2,1,0:T(8,128)(2,1)S(1)}, bf16[4,512,128]{2,1,0:T(8,128)(2,1)S(1)}, ...), condition=%wide.region_5.6_spmd, body=%wide.region_2.5_spmd.sunk | while | flops 546372608 | bytes 13903957 | solution.py:57
  372.0 30.4 %all_to_all.64 = bf16[8,256,256]{2,1,0:T(8,128)(2,1)S(1)} all-to-all(bf16[8,256,256]{2,1,0:T(8,128)(2,1)S(1)} %pad_maximum_fusion.1), channel_id=1, replica_groups=mesh['sp'=8,'dp'=4] {'sp'}, dimensions={0} | all-to-all | bytes 2097152 | tf_op jit(solution)/shard_map/all_to_all | solution.py:107
  403.0 6.8 %fusion.20 = bf16[1,256,2048]{2,1,0:T(8,128)(2,1)} fusion(bf16[256,2048]{0,1:T(8,128)(2,1)S(1)} %bitcast.95, bf16[2048,2048]{1,0:T(8,128)(2,1)} %all-gather.23.cloned.1.call-done), kind=kOutput, calls=%fused_computation.29 | convolution fusion | flops 2148007936 | bytes 10485760 | tf_op jit(solution)/shard_map/dot_general | solution.py:62
  (73 shorter events, 39.3 us)
Async XLA Ops:
  6.5 171.0 %copy-start = (bf16[1,256,2048]{2,1,0:T(8,128)(2,1)S(1)}, bf16[1,256,2048]{2,1,0:T(8,128)(2,1)}, u32[]{:S(2)}) copy-start(bf16[1,256,2048]{2,1,0:T(8,128)(2,1)} %param.13) | copy-start | bytes 3145732
  6.5 136.9 %copy-start.2 = (f32[2,128]{1,0:T(2,128)S(1)}, f32[2,128]{1,0:T(2,128)}, u32[]{:S(2)}) copy-start(f32[2,128]{1,0:T(2,128)} %param.18) | copy-start | bytes 3076
  6.5 45.0 %all-gather.17.cloned.1.call-start = ((), (), s32[]{:S(2)}) async-start(), calls=%async_computation.8 | async-start | bytes 1179648 | tf_op jit(solution)/shard_map/all_gather | solution.py:61
  7.3 95.7 %all-gather.9.cloned.1.call-start = ((), (), s32[]{:S(2)}) async-start(), calls=%async_computation.4 | async-start | bytes 2359296 | tf_op jit(solution)/shard_map/all_gather | solution.py:61
  8.0 134.6 %all-gather.13.cloned.1.call-start = ((), (), s32[]{:S(2)}) async-start(), calls=%async_computation.6 | async-start | bytes 1179648 | tf_op jit(solution)/shard_map/all_gather | solution.py:61
  8.7 168.8 %all-gather.19.cloned.1.call-start = ((), (), s32[]{:S(2)}) async-start(), calls=%async_computation.9 | async-start | bytes 5242880 | tf_op jit(solution)/shard_map/all_gather | solution.py:64
  51.6 185.7 %all-gather.11.cloned.1.call-start = ((), (), s32[]{:S(2)}) async-start(), calls=%async_computation.5 | async-start | bytes 10485760 | tf_op jit(solution)/shard_map/all_gather | solution.py:64
  103.0 170.2 %all-gather.15.cloned.1.call-start = ((), (), s32[]{:S(2)}) async-start(), calls=%async_computation.7 | async-start | bytes 5242880 | tf_op jit(solution)/shard_map/all_gather | solution.py:64
  142.7 198.4 %all-gather.21.cloned.1.call-start = ((), (), s32[]{:S(2)}) async-start(), calls=%async_computation.10 | async-start | bytes 2359296 | tf_op jit(solution)/shard_map/all_gather | solution.py:61
  182.6 83.5 %all-to-all-start.2 = ((bf16[256,8,128]{2,0,1:T(8,128)(2,1)}), bf16[256,8,128]{2,0,1:T(8,128)(2,1)}, u32[]{:S(2)}, u32[]{:S(2)}) async-start(bf16[256,8,128]{2,0,1:T(8,128)(2,1)} %bitcast.19), calls=%async_computation.2 | async-start | bytes 1048576 | tf_op jit(solution)/shard_map/all_to_all | solution.py:95
  266.1 40.1 %all-to-all-start = ((bf16[256,8,256]{0,2,1:T(8,128)(2,1)}), bf16[256,8,256]{0,2,1:T(8,128)(2,1)S(1)}, u32[]{:S(2)}, u32[]{:S(2)}) async-start(bf16[256,8,256]{0,2,1:T(8,128)(2,1)} %convert_element_type.44), calls=%async_computation | async-start | bytes 2097152 | tf_op jit(solution)/shard_map/all_to_all | solution.py:87
  306.2 35.5 %all-to-all-start.1 = ((bf16[256,8,128]{2,0,1:T(8,128)(2,1)}), bf16[256,8,128]{2,0,1:T(8,128)(2,1)S(1)}, u32[]{:S(2)}, u32[]{:S(2)}) async-start(bf16[256,8,128]{2,0,1:T(8,128)(2,1)} %bitcast.16), calls=%async_computation.1 | async-start | bytes 1048576 | tf_op jit(solution)/shard_map/all_to_all | solution.py:94
  309.7 93.2 %all-gather.23.cloned.1.call-start = ((), (), s32[]{:S(2)}) async-start(), calls=%async_computation.11 | async-start | bytes 10485760 | tf_op jit(solution)/shard_map/all_gather | solution.py:64
  403.0 6.8 %copy-start.1 = (bf16[1,256,2048]{2,1,0:T(8,128)(2,1)S(1)}, bf16[1,256,2048]{2,1,0:T(8,128)(2,1)}, u32[]{:S(2)}) copy-start(bf16[1,256,2048]{2,1,0:T(8,128)(2,1)} %param.13) | copy-start | bytes 3145732
Sparse Core Ops, SparseCore 0:
  9.4 42.1 all-gather.16
  53.6 49.3 all-gather.8
  105.0 37.5 all-gather.12
  144.0 33.4 all-gather.18
  179.0 58.2 all-gather.10
  238.7 34.4 all-gather.14
  275.2 65.8 all-gather.20
  342.6 57.7 all-gather.22
where the time goes:
time: 418 us; the launch traced here: 417 us
  waiting for transfers between devices  273 us (65%)
  matrix products  42.8 us (10%)
  blocking collectives  30.4 us (7%)
  local copies, waits for them, and re-layouts  27.8 us (7%)
  starting transfers between devices  14.8 us (4%)
  other arithmetic  14.5 us (3%)
  between operations  13.7 us (3%)
    all_gather x4, waiting for transfers between devices, project(): col_full = lax.all_gather(weight, 'sp', axis=1, tiled=True)  165 us
    all_gather x4, waiting for transfers between devices, project(): lax.all_gather(col_full, 'dp', axis=0, tiled=True)  84.5 us
    all_to_all x1, blocking collectives, on_device(): lax.all_to_all(mixed_heads, 'sp', split_axis=0, concat_axis=1, tiled=True)  30.4 us
    all_to_all x1, waiting for transfers between devices, on_device(): lax.all_to_all(prepare(raw_proj, qk_gain[0], cosine, sine_table).reshape(...  20.1 us
    dot_general x4, matrix products, project(): jnp.dot(own_rows, lax.all_gather(col_full, 'dp', axis=0, tiled=True), pre...  19.5 us
    dot_general x2, local copies, waits for them, and re-layouts, project(): jnp.dot(own_rows, lax.all_gather(col_full, 'dp', axis=0, tiled=True), pre...  18.7 us
    dot_general x8, matrix products, one_block(): jnp.dot(probs_bf, value_rows, preferred_element_type=jnp.float32)  17 us
  transfers between devices with their start and end apart: 11, of which 8 were waited for; matrix products, arithmetic and copies ran while one was open for 19% of the time, Pallas kernels for 0%

commit v1 on v0

--- a/solution.py
+++ b/solution.py
@@ -58,7 +58,7 @@
 
 
 def project(own_rows, weight):
-    col_full = lax.all_gather(weight, "sp", axis=1, tiled=True)
+    col_full = jnp.concatenate(lax.all_gather(weight, "sp"), 1)
     return jnp.dot(
         own_rows,
         lax.all_gather(col_full, "dp", axis=0, tiled=True),

time: 418 us -> 405 us (0.969)
  matrix products: 42.8 us -> 34.3 us
  local copies, waits for them, and re-layouts: 27.8 us -> 23.3 us
    dot_general x2 -> x0, local copies, waits for them, and re-layouts: 18.7 us -> none  [project(): jnp.dot(own_rows, lax.all_gather(col_full, 'dp', axis=0, tiled=True), pre...]
    reshape x0 -> x4, local copies, waits for them, and re-layouts: none -> 12.4 us  [project(): col_full = jnp.concatenate(lax.all_gather(weight, 'sp'), 1)]
    all_gather x4, waiting for transfers between devices: 84.5 us -> 94.6 us  [project(): lax.all_gather(col_full, 'dp', axis=0, tiled=True)]
    dot_general x8, matrix products: 17 us -> 8.4 us  [one_block(): jnp.dot(probs_bf, value_rows, preferred_element_type=jnp.float32)]
    all_to_all x1, waiting for transfers between devices: 20.1 us -> 13.2 us  [on_device(): lax.all_to_all(prepare(raw_proj, qk_gain[0], cosine, sine_table).reshape(...]
  transfers between devices with their start and end apart: 11 -> 11, of which waited for: 8 -> 9; matrix products, arithmetic and copies ran while one was open for 19% -> 16% of each run, Pallas kernels for 0% -> 0%
where the time goes in v1:
time: 405 us; the launch traced here: 404 us
  waiting for transfers between devices  273 us (67%)
  matrix products  34.3 us (8%)
  blocking collectives  28.8 us (7%)
  local copies, waits for them, and re-layouts  23.3 us (6%)
  other arithmetic  15.9 us (4%)
  starting transfers between devices  14.9 us (4%)
  between operations  13.7 us (3%)
    all_gather x4, waiting for transfers between devices, project(): col_full = jnp.concatenate(lax.all_gather(weight, 'sp'), 1)  163 us
    all_gather x4, waiting for transfers between devices, project(): lax.all_gather(col_full, 'dp', axis=0, tiled=True)  94.6 us
    all_to_all x1, blocking collectives, on_device(): lax.all_to_all(mixed_heads, 'sp', split_axis=0, concat_axis=1, tiled=True)  28.8 us
    dot_general x4, matrix products, project(): jnp.dot(own_rows, lax.all_gather(col_full, 'dp', axis=0, tiled=True), pre...  19.6 us
    all_to_all x1, waiting for transfers between devices, on_device(): lax.all_to_all(prepare(raw_proj, qk_gain[0], cosine, sine_table).reshape(...  13.2 us
    reshape x4, local copies, waits for them, and re-layouts, project(): col_full = jnp.concatenate(lax.all_gather(weight, 'sp'), 1)  12.4 us
    dot_general x8, matrix products, one_block(): jnp.dot(probs_bf, value_rows, preferred_element_type=jnp.float32)  8.4 us
  transfers between devices with their start and end apart: 11, of which 9 were waited for; matrix products, arithmetic and copies ran while one was open for 16% of the time, Pallas kernels for 0%

profile of v1, /device:TPU:0, one launch (start us, length us, event | category | flops | bytes accessed | tf_op | source)
XLA Modules:
  0.0 404.2 jit_solution(3382594581786282505)
XLA Ops:
  8.8 43.7 %all-gather.23.cloned.1.call-done = bf16[4096,128]{1,0:T(8,128)(2,1)} async-done(((bf16[512,128]{1,0:T(8,128)(2,1)}), bf16[4096,128]{1,0:T(8,128)(2,1)}) %all-gather.23.cloned.1.call-update) | async-done | bytes 1048592 | tf_op jit(solution)/shard_map/all_gather | solution.py:61
  54.8 47.6 %all-gather.21.cloned.1.call-done = bf16[4096,256]{1,0:T(8,128)(2,1)} async-done(((bf16[512,256]{1,0:T(8,128)(2,1)}), bf16[4096,256]{1,0:T(8,128)(2,1)}) %all-gather.21.cloned.1.call-update) | async-done | bytes 2097168 | tf_op jit(solution)/shard_map/all_gather | solution.py:61
  102.4 3.9 copy.19
  106.5 37.0 %all-gather.25.cloned.1.call-done = bf16[4096,128]{1,0:T(8,128)(2,1)} async-done(((bf16[512,128]{1,0:T(8,128)(2,1)}), bf16[4096,128]{1,0:T(8,128)(2,1)}) %all-gather.25.cloned.1.call-update) | async-done | bytes 1048592 | tf_op jit(solution)/shard_map/all_gather | solution.py:61
  146.9 31.2 %all-gather.15.cloned.1.call-done = bf16[2048,1024]{0,1:T(8,128)(2,1)} async-done(((bf16[512,1024]{0,1:T(8,128)(2,1)}), bf16[2048,1024]{0,1:T(8,128)(2,1)}) %all-gather.15.cloned.1.call-update) | async-done | bytes 4194320 | tf_op jit(solution)/shard_map/all_gather | solution.py:64
  178.0 3.5 multiply_reduce_fusion.3
  184.5 5.5 %all-to-all-start.1 = ((bf16[256,8,128]{2,0,1:T(8,128)(2,1)}), bf16[256,8,128]{2,0,1:T(8,128)(2,1)S(1)}, u32[]{:S(2)}, u32[]{:S(2)}) async-start(bf16[256,8,128]{2,0,1:T(8,128)(2,1)} %bitcast.22), calls=%async_computation.1 | async-start | bytes 1048576 | tf_op jit(solution)/shard_map/all_to_all | solution.py:94
  190.0 47.8 %all-gather.13.cloned.1.call-done = bf16[2048,2048]{0,1:T(8,128)(2,1)} async-done(((bf16[512,2048]{0,1:T(8,128)(2,1)}), bf16[2048,2048]{0,1:T(8,128)(2,1)}) %all-gather.13.cloned.1.call-update) | async-done | bytes 8388624 | tf_op jit(solution)/shard_map/all_gather | solution.py:64
  237.7 5.8 %multiply_reduce_fusion.2 = (f32[256,16]{0,1:T(8,128)S(1)}, f32[256,16,128]{0,2,1:T(8,128)S(1)}) fusion(bf16[16,128,2048]{2,1,0:T(8,128)(2,1)} %bitcast.131, bf16[1,256,2048]{2,1,0:T(8,128)(2,1)S(1)} %copy-done), kind=kOutput, calls=%fused_computation.31 | convolution fusion | flops 2148528128 | bytes 11550720 | tf_op jit(solution)/shard_map/dot_general | solution.py:62
  245.2 3.6 reshape.191
  248.8 4.3 %subtract_convert_fusion = (bf16[256,16,64,1]{0,3,2,1:T(2,128)(2,1)S(1)}, bf16[256,16,64,1]{0,3,2,1:T(2,128)(2,1)S(1)}) fusion(f32[256,16,64,2]{0,3,2,1:T(2,128)} %reshape.191, f32[256,64]{0,1:T(8,128)S(1)} %get-tuple-element.92, f32[256,64]{0,1:T(8,128)S(1)} %get-tuple-element.91), kind=kLoop, calls=%fused_computation.44 | loop fusion | flops 2097152 | bytes 3276800 | tf_op jit(solution)/shard_map/convert.2
  253.1 2.4 pad_maximum_fusion
  256.8 5.6 %all-to-all-start = ((bf16[256,8,256]{0,2,1:T(8,128)(2,1)}), bf16[256,8,256]{0,2,1:T(8,128)(2,1)S(1)}, u32[]{:S(2)}, u32[]{:S(2)}) async-start(bf16[256,8,256]{0,2,1:T(8,128)(2,1)} %convert_element_type.44), calls=%async_computation | async-start | bytes 2097152 | tf_op jit(solution)/shard_map/all_to_all | solution.py:87
  262.4 11.3 %all-gather.17.cloned.1.call-done = bf16[2048,1024]{0,1:T(8,128)(2,1)} async-done(((bf16[512,1024]{0,1:T(8,128)(2,1)}), bf16[2048,1024]{0,1:T(8,128)(2,1)}) %all-gather.17.cloned.1.call-update) | async-done | bytes 4194320 | tf_op jit(solution)/shard_map/all_gather | solution.py:64
  273.7 3.5 fusion.21
  278.6 13.2 %all-to-all-done = bf16[256,8,256]{0,2,1:T(8,128)(2,1)S(1)} async-done(((bf16[256,8,256]{0,2,1:T(8,128)(2,1)}), bf16[256,8,256]{0,2,1:T(8,128)(2,1)S(1)}, u32[]{:S(2)}, u32[]{:S(2)}) %all-to-all-start) | async-done | bytes 1048608 | tf_op jit(solution)/shard_map/all_to_all | solution.py:87
  291.8 3.5 all-to-all-start.2
  295.4 34.2 %all-gather.27.cloned.1.call-done = bf16[4096,256]{1,0:T(8,128)(2,1)} async-done(((bf16[512,256]{1,0:T(8,128)(2,1)}), bf16[4096,256]{1,0:T(8,128)(2,1)}) %all-gather.27.cloned.1.call-update) | async-done | bytes 2097168 | tf_op jit(solution)/shard_map/all_gather | solution.py:61
  329.6 4.0 copy.28
  335.1 10.8 %while.20 = (s32[]{:T(128)}, bf16[4,512,128]{2,1,0:T(8,128)(2,1)S(1)}, bf16[4,512,128]{2,1,0:T(8,128)(2,1)S(1)}, bf16[2048,128]{1,0:T(8,128)(2,1)S(1)}, bf16[2048,128]{1,0:T(8,128)(2,1)}, /*index=5*/s32[]{:T(128)}) while((s32[]{:T(128)}, bf16[4,512,128]{2,1,0:T(8,128)(2,1)S(1)}, bf16[4,512,128]{2,1,0:T(8,128)(2,1)S(1)}, ...), condition=%wide.region_5.6_spmd, body=%wide.region_2.5_spmd.sunk | while | flops 546372608 | bytes 16001129 | solution.py:57
  345.9 10.8 %while.21 = (s32[]{:T(128)}, bf16[4,512,128]{2,1,0:T(8,128)(2,1)S(1)}, bf16[4,512,128]{2,1,0:T(8,128)(2,1)S(1)}, bf16[2048,128]{1,0:T(8,128)(2,1)S(1)}, bf16[2048,128]{1,0:T(8,128)(2,1)}, /*index=5*/s32[]{:T(128)}) while((s32[]{:T(128)}, bf16[4,512,128]{2,1,0:T(8,128)(2,1)S(1)}, bf16[4,512,128]{2,1,0:T(8,128)(2,1)S(1)}, ...), condition=%wide.region_9.10_spmd, body=%wide.region_6.9_spmd.sunk | while | flops 546372608 | bytes 16001129 | solution.py:57
  356.9 28.8 %all_to_all.64 = bf16[8,256,256]{2,1,0:T(8,128)(2,1)S(1)} all-to-all(bf16[8,256,256]{2,1,0:T(8,128)(2,1)S(1)} %pad_maximum_fusion.1), channel_id=1, replica_groups=mesh['sp'=8,'dp'=4] {'sp'}, dimensions={0} | all-to-all | bytes 2097152 | tf_op jit(solution)/shard_map/all_to_all | solution.py:107
  386.1 4.4 %all-gather.19.cloned.1.call-done = bf16[2048,2048]{0,1:T(8,128)(2,1)} async-done(((bf16[512,2048]{0,1:T(8,128)(2,1)}), bf16[2048,2048]{0,1:T(8,128)(2,1)}) %all-gather.19.cloned.1.call-update) | async-done | bytes 8388624 | tf_op jit(solution)/shard_map/all_gather | solution.py:64
  390.5 6.8 %fusion.20 = bf16[1,256,2048]{2,1,0:T(8,128)(2,1)} fusion(bf16[256,2048]{0,1:T(8,128)(2,1)S(1)} %bitcast.129, bf16[2048,2048]{0,1:T(8,128)(2,1)} %all-gather.19.cloned.1.call-done), kind=kOutput, calls=%fused_computation.29 | convolution fusion | flops 2148007936 | bytes 10485760 | tf_op jit(solution)/shard_map/dot_general | solution.py:62
  (93 shorter events, 38.8 us)
Async XLA Ops:
  6.5 171.5 %copy-start = (bf16[1,256,2048]{2,1,0:T(8,128)(2,1)S(1)}, bf16[1,256,2048]{2,1,0:T(8,128)(2,1)}, u32[]{:S(2)}) copy-start(bf16[1,256,2048]{2,1,0:T(8,128)(2,1)} %param.13) | copy-start | bytes 3145732
  6.5 46.0 %all-gather.23.cloned.1.call-start = ((), (), s32[]{:S(2)}) async-start(), calls=%async_computation.9 | async-start | bytes 1179648 | tf_op jit(solution)/shard_map/all_gather | solution.py:61
  7.3 95.2 %all-gather.21.cloned.1.call-start = ((), (), s32[]{:S(2)}) async-start(), calls=%async_computation.8 | async-start | bytes 2359296 | tf_op jit(solution)/shard_map/all_gather | solution.py:61
  8.0 135.4 %all-gather.25.cloned.1.call-start = ((), (), s32[]{:S(2)}) async-start(), calls=%async_computation.10 | async-start | bytes 1179648 | tf_op jit(solution)/shard_map/all_gather | solution.py:61
  8.7 169.3 %all-gather.15.cloned.1.call-start = ((), (), s32[]{:S(2)}) async-start(), calls=%async_computation.5 | async-start | bytes 5242880 | tf_op jit(solution)/shard_map/all_gather | solution.py:64
  54.8 183.0 %all-gather.13.cloned.1.call-start = ((), (), s32[]{:S(2)}) async-start(), calls=%async_computation.4 | async-start | bytes 10485760 | tf_op jit(solution)/shard_map/all_gather | solution.py:64
  102.4 44.1 %copy-start.5 = (f32[2,128]{1,0:T(2,128)S(1)}, f32[2,128]{1,0:T(2,128)}, u32[]{:S(2)}) copy-start(f32[2,128]{1,0:T(2,128)} %param.18) | copy-start | bytes 3076
  106.4 167.2 %all-gather.17.cloned.1.call-start = ((), (), s32[]{:S(2)}) async-start(), calls=%async_computation.6 | async-start | bytes 5242880 | tf_op jit(solution)/shard_map/all_gather | solution.py:64
  145.7 183.9 %all-gather.27.cloned.1.call-start = ((), (), s32[]{:S(2)}) async-start(), calls=%async_computation.11 | async-start | bytes 2359296 | tf_op jit(solution)/shard_map/all_gather | solution.py:61
  184.5 72.4 %all-to-all-start.1 = ((bf16[256,8,128]{2,0,1:T(8,128)(2,1)}), bf16[256,8,128]{2,0,1:T(8,128)(2,1)S(1)}, u32[]{:S(2)}, u32[]{:S(2)}) async-start(bf16[256,8,128]{2,0,1:T(8,128)(2,1)} %bitcast.22), calls=%async_computation.1 | async-start | bytes 1048576 | tf_op jit(solution)/shard_map/all_to_all | solution.py:94
  256.8 35.0 %all-to-all-start = ((bf16[256,8,256]{0,2,1:T(8,128)(2,1)}), bf16[256,8,256]{0,2,1:T(8,128)(2,1)S(1)}, u32[]{:S(2)}, u32[]{:S(2)}) async-start(bf16[256,8,256]{0,2,1:T(8,128)(2,1)} %convert_element_type.44), calls=%async_computation | async-start | bytes 2097152 | tf_op jit(solution)/shard_map/all_to_all | solution.py:87
  291.8 42.4 %all-to-all-start.2 = ((bf16[256,8,128]{2,0,1:T(8,128)(2,1)}), bf16[256,8,128]{2,0,1:T(8,128)(2,1)S(1)}, u32[]{:S(2)}, u32[]{:S(2)}) async-start(bf16[256,8,128]{2,0,1:T(8,128)(2,1)} %bitcast.28), calls=%async_computation.2 | async-start | bytes 1048576 | tf_op jit(solution)/shard_map/all_to_all | solution.py:95
  295.3 95.2 %all-gather.19.cloned.1.call-start = ((), (), s32[]{:S(2)}) async-start(), calls=%async_computation.7 | async-start | bytes 10485760 | tf_op jit(solution)/shard_map/all_gather | solution.py:64
  334.2 0.8 copy-start.2
  335.1 1.6 copy-start.3
  337.8 1.6 copy-start.3
  340.5 1.6 copy-start.3
  343.2 1.6 copy-start.3
  345.9 1.6 copy-start.4
  348.6 1.6 copy-start.4
  351.3 1.6 copy-start.4
  354.0 1.6 copy-start.4
  390.5 6.8 %copy-start.1 = (bf16[1,256,2048]{2,1,0:T(8,128)(2,1)S(1)}, bf16[1,256,2048]{2,1,0:T(8,128)(2,1)}, u32[]{:S(2)}) copy-start(bf16[1,256,2048]{2,1,0:T(8,128)(2,1)} %param.13) | copy-start | bytes 3145732
Sparse Core Ops, SparseCore 0:
  9.5 42.9 all-gather.22
  54.6 47.7 all-gather.20
  104.6 38.7 all-gather.24
  144.8 33.1 all-gather.14
  179.4 58.2 all-gather.12
  239.2 34.4 all-gather.16
  275.8 53.7 all-gather.26
  333.7 56.7 all-gather.18
